TPU v7x, 128 devices: a whole 4x4x4 slice. The times are simulated.
128 devices in a mesh: sp: 32 (over z, y, core), tp: 4 (over x).
Axes of the slice: x: 4, y: 4, z: 4, core: 2. Of those that a mesh axis runs over, the one named last changes fastest.
Arguments:
- tokens: bfloat16 [32768, 2048], P('sp', 'tp'), may hold values from -6 to 6
- input_norm_gain: float32 [2048], replicated, may hold values from 0.1 to 1.9
- pooling_input_matrix: bfloat16 [2048, 512], P(None, 'tp'), may hold values from -0.125 to 0.125
- query_projection_matrix: bfloat16 [2048, 1024], P(None, 'tp'), may hold values from -0.125 to 0.125
- key_projection_matrix: bfloat16 [2048, 1024], P(None, 'tp'), may hold values from -0.125 to 0.125
- value_projection_matrix: bfloat16 [2048, 1024], P(None, 'tp'), may hold values from -0.125 to 0.125
- output_gate_matrix: bfloat16 [2048, 1024], P(None, 'tp'), may hold values from -0.125 to 0.125
- input_gate_matrix: bfloat16 [2048, 2, 8], replicated
- forget_gate_matrix: bfloat16 [2048, 2, 8], replicated, may hold values from -0.125 to 0.125
- forget_gate_bias: float32 [2, 8], replicated
- log_forget_scale: float32 [2, 32768], P(None, 'sp'), may hold values from 0.35 to 2.8
- extra_log_forget: float32 [2, 32768], P(None, 'sp'), may hold values from -0.7 to 0, as said below
- starting_memory: float32 [2, 8, 128, 128], P(None, 'tp'), may hold values from -3 to 3
- starting_normalizer: float32 [2, 8, 128], P(None, 'tp'), may hold values from -3 to 3
- starting_log_scale: float32 [2, 8], P(None, 'tp'), may hold values from 2 to 5
- pooling_group_map: bfloat16 [4, 128, 128], replicated, may hold values from -0.5 to 0.5
- pooling_channel_scale: float32 [512], replicated, may hold values from 0.1 to 1.9
- memory_head_gain: float32 [1024], replicated, may hold values from 0.1 to 1.9
- pooling_output_matrix: bfloat16 [512, 2048], replicated, may hold values from -0.25 to 0.25
- memory_output_matrix: bfloat16 [1024, 2048], replicated, may hold values from -0.1875 to 0.1875
Outputs:
- mixed_out: bfloat16 [32768, 2048], P(('sp', 'tp'))
Inputs may be any that keep to these rules, and one draw needn't show every extreme that they name: `extra_log_forget`: at most three nonzero entries in each direction.
All inputs are finite; a program needn't handle non-finite values.
Results may differ from a plain program's by a relative error of at most 0.0091.
Values may be sent and summed in bfloat16 or wider, within the bound.
A program may use at most 128 MiB of HBM per device.

v0:
```python
import jax
import jax.numpy as jnp
from jax import lax
from jax.sharding import PartitionSpec as P

DH = 128
BLOCK = 128


NEG_BIG = -1e30
LN_EPS = 1e-05
HEAD_EPS = 1e-06
RIM_ROWS = 8


def extended(block, sides, width):
    for axis, dim in sides:
        count = lax.axis_size(axis)
        forward = [(i, i + 1) for i in range(count - 1)]
        backward = [(target, source) for source, target in forward]
        low = lax.ppermute(
            lax.slice_in_dim(block, block.shape[dim] - width, None, axis=dim), axis, forward
        )
        high = lax.ppermute(lax.slice_in_dim(block, 0, width, axis=dim), axis, backward)
        block = jnp.concatenate([low, block, high], axis=dim)
    return block


def block_step(carried, pieces):
    memory, normer, maxlog = carried
    q_blk, k_blk, v_blk, i_blk, f_blk = pieces
    lower_mask = jnp.tril(jnp.ones((BLOCK, BLOCK), dtype=bool))
    cumulative = jnp.cumsum(f_blk, axis=-1)
    exponent = jnp.where(
        lower_mask, cumulative[:, :, None] - cumulative[:, None, :] + i_blk[:, None, :], NEG_BIG
    )
    carried_log = cumulative + maxlog[:, None]
    row_max = jnp.maximum(carried_log, exponent.max(-1))
    fading = jnp.exp(carried_log - row_max)
    scores = jnp.einsum("htd,hsd->hts", q_blk, k_blk) * jnp.exp(exponent - row_max[:, :, None])
    numerator = fading[:, :, None] * jnp.einsum("hvk,htk->htv", memory, q_blk) + jnp.einsum(
        "hts,hsv->htv", scores, v_blk
    )
    denominator = fading * jnp.einsum("hk,htk->ht", normer, q_blk) + scores.sum(-1)
    summed = cumulative[:, -1]
    weight_log = summed[:, None] - cumulative + i_blk
    new_max = jnp.maximum(summed + maxlog, weight_log.max(-1))
    carry_scale = jnp.exp(summed + maxlog - new_max)
    weights = jnp.exp(weight_log - new_max[:, None])
    memory = carry_scale[:, None, None] * memory + jnp.einsum(
        "hsv,hsk->hvk", v_blk * weights[:, :, None], k_blk
    )
    normer = carry_scale[:, None] * normer + jnp.einsum("hs,hsk->hk", weights, k_blk)
    return ((memory, normer, new_max), (numerator, denominator, row_max))


def to_blocks(source):
    return jnp.moveaxis(
        source.reshape((source.shape[0], source.shape[1] // BLOCK, BLOCK) + source.shape[2:]), 1, 0
    )


def from_blocks(source):
    return jnp.moveaxis(source, 0, 1).reshape(
        (source.shape[1], source.shape[0] * source.shape[2]) + source.shape[3:]
    )


def local_pass(query_heads, key_heads, value_heads, log_in, log_forget_gate):
    head_count = query_heads.shape[0]
    head_size = query_heads.shape[2]
    initial = (
        jnp.zeros((head_count, head_size, head_size), jnp.float32),
        jnp.zeros((head_count, head_size), jnp.float32),
        jnp.full((head_count,), NEG_BIG, jnp.float32),
    )
    finals, outputs = lax.scan(
        block_step,
        initial,
        tuple(
            (
                to_blocks(member)
                for member in (query_heads, key_heads, value_heads, log_in, log_forget_gate)
            )
        ),
    )
    numerator, denominator, row_max = (from_blocks(member) for member in outputs)
    falls = jnp.cumsum(log_forget_gate, axis=1)
    return ((falls[:, -1],) + finals, (numerator, denominator, row_max, falls))


def join_states(earlier, later):
    early_fall, early_memory, early_normer, early_max = earlier
    late_fall, late_memory, late_normer, late_max = later
    merged_max = jnp.maximum(early_max + late_fall, late_max)
    early_weight = jnp.exp(early_max + late_fall - merged_max)
    late_weight = jnp.exp(late_max - merged_max)
    return (
        late_fall,
        early_weight[..., None, None] * early_memory + late_weight[..., None, None] * late_memory,
        early_weight[..., None] * early_normer + late_weight[..., None] * late_normer,
        merged_max,
    )


def prefix_from_all(gathered, position, from_later):
    falls, memories, normers, maxima = gathered
    order = jnp.arange(falls.shape[0], dtype=jnp.int32)
    inclusive = jnp.cumsum(falls, axis=0)
    exclusive = inclusive - falls
    if from_later:
        valid = order > position
        between = exclusive - inclusive[position][None]
        total_fall = inclusive[-1] - inclusive[position]
    else:
        valid = order < position
        between = exclusive[position][None] - inclusive
        total_fall = exclusive[position]
    log_weight = jnp.where(valid[:, None], maxima + between, NEG_BIG)
    joint_max = jnp.max(log_weight, axis=0)
    weights = jnp.where(valid[:, None], jnp.exp(log_weight - joint_max[None]), 0.0)
    memory = jnp.einsum("jh,jhvk->hvk", weights, memories)
    normer = jnp.einsum("jh,jhk->hk", weights, normers)
    return (total_fall, memory, normer, joint_max)


def finish(local_terms, entering, query_heads):
    numerator, denominator, row_max, falls = local_terms
    fall_in, memory, normer, max_in = entering
    state_log = falls + max_in[:, None]
    joint_max = jnp.maximum(row_max, state_log)
    local_weight = jnp.exp(row_max - joint_max)
    state_weight = jnp.exp(state_log - joint_max)
    full_numerator = local_weight[..., None] * numerator + state_weight[..., None] * jnp.einsum(
        "hvk,htk->htv", memory, query_heads
    )
    full_denominator = local_weight * denominator + state_weight * jnp.einsum(
        "hk,htk->ht", normer, query_heads
    )
    return full_numerator / jnp.maximum(jnp.abs(full_denominator), 1.0)[..., None]


def per_device(
    tokens,
    input_norm_gain,
    pooling_input_matrix,
    query_projection_matrix,
    key_projection_matrix,
    value_projection_matrix,
    output_gate_matrix,
    input_gate_matrix,
    forget_gate_matrix,
    forget_gate_bias,
    log_forget_scale,
    extra_log_forget,
    starting_memory,
    starting_normalizer,
    starting_log_scale,
    pooling_group_map,
    pooling_channel_scale,
    memory_head_gain,
    pooling_output_matrix,
    memory_output_matrix,
):
    local_rows = tokens.shape[0]
    own_width = tokens.shape[1]
    model_width = own_width * lax.axis_size("tp")
    group_index = lax.axis_index("tp")
    seq_index = lax.axis_index("sp")
    group_dim = pooling_input_matrix.shape[1]
    head_local = query_projection_matrix.shape[1] // DH
    mem_width = head_local * DH
    main_weight = jnp.concatenate(
        [
            pooling_input_matrix,
            query_projection_matrix,
            key_projection_matrix,
            value_projection_matrix,
            output_gate_matrix,
        ],
        axis=1,
    )
    gate_in = lax.dynamic_slice_in_dim(input_gate_matrix, group_index * head_local, head_local, 2)
    gate_fg = lax.dynamic_slice_in_dim(forget_gate_matrix, group_index * head_local, head_local, 2)
    gate_weight = jnp.concatenate([gate_in, gate_fg], axis=1).reshape(model_width, 4 * head_local)
    whole_rows = lax.all_gather(tokens, "tp", axis=1, tiled=True)
    floats = whole_rows.astype(jnp.float32)
    mean_row = jnp.sum(floats, axis=1) / model_width
    variance = jnp.sum(floats * floats, axis=1) / model_width - mean_row * mean_row
    normed = (
        (floats - mean_row[:, None]) * lax.rsqrt(variance + LN_EPS)[:, None] * input_norm_gain
    ).astype(jnp.bfloat16)
    projected = jnp.dot(normed, main_weight, preferred_element_type=jnp.float32)
    gate_pre = jnp.dot(normed, gate_weight, preferred_element_type=jnp.float32)
    pool_in = projected[:, :group_dim].astype(jnp.bfloat16)
    queries = projected[:, group_dim : group_dim + mem_width].astype(jnp.bfloat16)
    key_rows = projected[:, group_dim + mem_width : group_dim + 2 * mem_width].astype(jnp.bfloat16)
    value_rows = projected[:, group_dim + 2 * mem_width : group_dim + 3 * mem_width].astype(
        jnp.bfloat16
    )
    out_gate = projected[:, group_dim + 3 * mem_width :].astype(jnp.bfloat16)
    gate_pre = gate_pre.reshape(local_rows, 2, 2, head_local)
    log_in = gate_pre[:, 0]
    bias_own = lax.dynamic_slice_in_dim(forget_gate_bias, group_index * head_local, head_local, 1)
    log_forget_gate = (
        jax.nn.log_sigmoid(gate_pre[:, 1] + bias_own[None]) * log_forget_scale.T[:, :, None]
        + extra_log_forget.T[:, :, None]
    )

    def heads_of(source, factor):
        return (
            (source.astype(jnp.float32) * factor)
            .reshape(local_rows, head_local, DH)
            .transpose(1, 0, 2)
        )

    query_heads = heads_of(queries, 1.0)
    key_heads = heads_of(key_rows, DH ** (-0.5))
    value_heads = heads_of(value_rows, 1.0)
    forward_summary, forward_local = local_pass(
        query_heads, key_heads, value_heads, log_in[:, 0].T, log_forget_gate[:, 0].T
    )
    flipped_query = query_heads[:, ::-1]
    backward_summary, backward_local = local_pass(
        flipped_query,
        key_heads[:, ::-1],
        value_heads[:, ::-1],
        log_in[:, 1].T[:, ::-1],
        log_forget_gate[:, 1].T[:, ::-1],
    )
    rimmed = extended(pool_in, (("sp", 0),), RIM_ROWS).astype(jnp.float32)
    half_span = jnp.left_shift(jnp.int32(1), group_index)
    grouped = pool_in.astype(jnp.float32)
    pooled = jnp.zeros_like(grouped)
    for offset in range(-RIM_ROWS, RIM_ROWS):
        inside = ((offset >= -half_span) & (offset < half_span)).astype(jnp.float32)
        pooled = pooled + inside * rimmed[RIM_ROWS + offset : RIM_ROWS + offset + local_rows]
    positions = seq_index * local_rows + jnp.arange(local_rows, dtype=jnp.int32)
    total_rows = local_rows * lax.axis_size("sp")
    counts = (
        jnp.minimum(positions + half_span, total_rows) - jnp.maximum(positions - half_span, 0)
    ).astype(jnp.float32)
    contrast = (pooled / counts[:, None] - grouped).astype(jnp.bfloat16)
    map_own = lax.dynamic_index_in_dim(pooling_group_map, group_index, 0, keepdims=False)
    scale_own = lax.dynamic_slice_in_dim(
        pooling_channel_scale, group_index * group_dim, group_dim, 0
    )
    pool_out = (jnp.dot(contrast, map_own, preferred_element_type=jnp.float32) * scale_own).astype(
        jnp.bfloat16
    )
    stacked = tuple(
        (
            jnp.stack([forward_part, backward_part])[None]
            for forward_part, backward_part in zip(forward_summary, backward_summary)
        )
    )
    gathered = lax.all_gather(stacked, "sp", axis=0, tiled=True)
    forward_prefix = prefix_from_all(tuple((member[:, 0] for member in gathered)), seq_index, False)
    backward_prefix = prefix_from_all(tuple((member[:, 1] for member in gathered)), seq_index, True)

    def initial_state(direction):
        return (
            jnp.zeros((head_local,), jnp.float32),
            starting_memory[direction],
            starting_normalizer[direction],
            starting_log_scale[direction],
        )

    forward = finish(forward_local, join_states(initial_state(0), forward_prefix), query_heads)
    backward = finish(backward_local, join_states(initial_state(1), backward_prefix), flipped_query)
    hidden = forward + backward[:, ::-1]
    head_mean = jnp.mean(hidden, axis=-1, keepdims=True)
    head_var = jnp.mean(jnp.square(hidden - head_mean), axis=-1, keepdims=True)
    gain_heads = lax.dynamic_slice_in_dim(
        memory_head_gain, group_index * mem_width, mem_width, 0
    ).reshape(head_local, DH)
    scaled = (hidden - head_mean) * lax.rsqrt(head_var + HEAD_EPS) * gain_heads[:, None, :]
    mem_out = (
        scaled.transpose(1, 0, 2).reshape(local_rows, mem_width)
        * jax.nn.sigmoid(out_gate.astype(jnp.float32))
    ).astype(jnp.bfloat16)
    mixed = jnp.concatenate([pool_out, mem_out], axis=1)
    owned = lax.all_to_all(mixed, "tp", split_axis=0, concat_axis=1, tiled=True)
    owner_rows = owned.shape[0]
    owned = owned.reshape(owner_rows, lax.axis_size("tp"), group_dim + mem_width)
    pool_part = owned[:, :, :group_dim].reshape(owner_rows, lax.axis_size("tp") * group_dim)
    mem_part = owned[:, :, group_dim:].reshape(owner_rows, lax.axis_size("tp") * mem_width)
    result = jnp.dot(
        pool_part, pooling_output_matrix, preferred_element_type=jnp.float32
    ) + jnp.dot(mem_part, memory_output_matrix, preferred_element_type=jnp.float32)
    return result.astype(jnp.bfloat16)


def solution(mesh):
    placed = (
        P("sp", "tp"),
        P(),
        P(None, "tp"),
        P(None, "tp"),
        P(None, "tp"),
        P(None, "tp"),
        P(None, "tp"),
        P(),
        P(),
        P(),
        P(None, "sp"),
        P(None, "sp"),
        P(None, "tp", None, None),
        P(None, "tp", None),
        P(None, "tp"),
        P(),
        P(),
        P(),
        P(),
        P(),
    )
    return jax.shard_map(
        per_device, mesh=mesh, in_specs=placed, out_specs=P(("sp", "tp"), None), check_vma=False
    )
```

profile of v0, /device:TPU:1, one launch (start us, length us, event | category | flops | bytes accessed | tf_op | source)
XLA Modules:
  0.0 383.7 jit_solution(3305362146877481871)
XLA Ops:
  9.4 1.9 constant_dynamic-update-slice_fusion.8
  11.3 2.3 constant_dynamic-update-slice_fusion.7
  16.9 43.3 %all-gather.9.cloned.1.call-done = bf16[1024,2048]{1,0:T(8,128)(2,1)} async-done(((bf16[1024,512]{1,0:T(8,128)(2,1)}), bf16[1024,2048]{1,0:T(8,128)(2,1)}) %all-gather.9.cloned.1.call-update) | async-done | bytes 4194320 | tf_op jit(solution)/shard_map/all_gather | solution.py:186
  60.2 3.6 convert_reduce_fusion
  63.9 8.5 %convolution_convert_fusion = bf16[1024,1152]{1,0:T(8,128)(2,1)S(1)} fusion(bf16[2048,1152]{1,0:T(8,128)(2,1)} %constant_dynamic-update-slice_fusion.4, bf16[1024,2048]{1,0:T(8,128)(2,1)S(1)} %copy-done.5, f32[2048]{0:T(1024)S(1)} %copy-done.21, f32[1024]{0:T(1024)S(1)} %get-tuple-element.398, f32[1024]{0:T(1024)S(1)} %get-tuple-element.397), kind=kOutput, calls=%fused_computation.125 | convolution fusion | flops 4843503616 | bytes 11288576 | tf_op jit(solution)/shard_map/dot_general | solution.py:193
  72.4 1.5 multiply_bitcast_fusion
  74.7 1.3 copy_bitcast_fusion
  75.9 5.1 %rev.22 = bf16[2,1024,128]{2,1,0:T(8,128)(2,1)} reverse(bf16[2,1024,128]{2,1,0:T(8,128)(2,1)S(1)} %get-tuple-element.407), dimensions={1} | reverse | bytes 1048576 | tf_op jit(solution)/shard_map/rev | solution.py:223
  81.0 3.7 fusion.70
  86.3 1.3 copy.211
  87.6 5.1 %rev.20 = f32[2,1024,128]{2,1,0:T(8,128)} reverse(f32[2,1024,128]{2,1,0:T(8,128)S(1)} %bitcast.498), dimensions={1} | reverse | bytes 2097152 | tf_op jit(solution)/shard_map/rev | solution.py:227
  92.7 8.2 %rev.21 = bf16[2,1024,128]{2,1,0:T(8,128)(2,1)} reverse(bf16[2,1024,128]{2,1,0:T(8,128)(2,1)} %get-tuple-element.381), dimensions={1} | reverse | bytes 1048576 | tf_op jit(solution)/shard_map/rev | solution.py:226
  101.0 1.9 copy.212
  104.0 66.0 %while.43 = (s32[]{:T(128)}, f32[2,128,128]{2,1,0:T(8,128)S(1)}, f32[2,128]{1,0:T(2,128)S(1)}, f32[2]{0:T(128)S(1)}, f32[8,2,128,128]{3,2,1,0:T(8,128)}, /*index...) while((s32[]{:T(128)}, f32[2,128,128]{2,1,0:T(8,128)S(1)}, ...), condition=%wide.region_18.19_spmd.clone, body=%wide.region_13.18_spmd.clone.sunk | while | flops 34327816 | bytes 1600317 | solution.py:77
  110.4 1.8 fusion.266
  118.7 1.8 fusion.266
  126.9 1.8 fusion.266
  135.1 1.8 fusion.266
  143.4 1.8 fusion.266
  151.6 1.8 fusion.266
  159.9 1.8 fusion.266
  168.1 1.8 fusion.266
  169.9 1.9 copy.213
  172.9 58.1 %while.42 = (s32[]{:T(128)}, f32[2,128,128]{2,1,0:T(8,128)S(1)}, f32[2,128]{1,0:T(2,128)S(1)}, f32[2]{0:T(128)S(1)}, f32[8,2,128,128]{3,2,1,0:T(8,128)}, /*index...) while((s32[]{:T(128)}, f32[2,128,128]{2,1,0:T(8,128)S(1)}, ...), condition=%wide.region_7.8_spmd.clone, body=%wide.region_2.7_spmd.clone.sunk | while | flops 34327816 | bytes 1600821 | solution.py:77
  231.8 1.3 dynamic_slice.60
  236.3 25.2 %all-gather.4 = f32[32,2,2]{2,1,0:T(2,128)S(1)} all-gather(f32[1,2,2]{2,1,0:T(2,128)S(1)} %maximum_bitcast_fusion), channel_id=2, replica_groups=mesh['sp'=32,'tp'=4] {'sp'}, dimensions={0}, use_global_device_ids=true | all-gather | bytes 528 | tf_op jit(solution)/shard_map/all_gather | solution.py:257
  261.7 23.6 %all-gather.5 = f32[32,2,2]{2,1,0:T(2,128)S(1)} all-gather(f32[1,2,2]{2,1,0:T(2,128)S(1)} %maximum_bitcast_fusion.1), channel_id=3, replica_groups=mesh['sp'=32,'tp'=4] {'sp'}, dimensions={0}, use_global_device_ids=true | all-gather | bytes 528 | tf_op jit(solution)/shard_map/all_gather | solution.py:257
  286.8 2.1 collective-permute-start.1
  288.9 3.5 collective-permute-start
  292.4 22.6 %all-gather.3 = bf16[64,2,128]{2,1,0:T(2,128)(2,1)S(1)} all-gather(bf16[2,2,128]{2,1,0:T(2,128)(2,1)S(1)} %pad_maximum_fusion.3), channel_id=5, replica_groups=mesh['sp'=32,'tp'=4] {'sp'}, dimensions={0}, use_global_device_ids=true | all-gather | bytes 33792 | tf_op jit(solution)/shard_map/all_gather | solution.py:257
  315.6 1.3 fusion.177
  317.0 1.3 fusion.83
  318.4 2.6 copy.115
  321.0 2.4 reshape.649
  323.6 1.3 copy.109
  324.9 2.4 reshape.646
  327.4 2.1 fusion.82
  329.5 4.2 %slice_bitcast_fusion.1 = (bf16[32,2,128,128]{3,2,1,0:T(8,128)(2,1)}, bf16[32,2,128,128]{3,2,1,0:T(8,128)(2,1)S(1)}) fusion(bf16[32,2,2,128,128]{4,3,2,1,0:T(8,128)(2,1)} %bitcast.502), kind=kLoop, calls=%fused_computation.118 | loop fusion | bytes 8388608 | tf_op jit(solution)/shard_map/squeeze | solution.py:258
  333.7 1.2 fusion.72
  335.0 1.3 fusion.81
  336.4 9.4 %rev.23 = f32[2,1024,128]{1,2,0:T(8,128)} reverse(f32[2,1024,128]{1,2,0:T(8,128)} %fusion.81), dimensions={1} | reverse | bytes 2097152 | tf_op jit(solution)/shard_map/rev | solution.py:271
  345.7 2.8 fusion.74
  348.6 2.0 fusion.176
  351.9 1.6 copy.152
  353.4 1.3 multiply_convert_fusion
  356.0 15.5 %all_to_all.16 = bf16[4,256,384]{1,2,0:T(8,128)(2,1)S(1)} all-to-all(bf16[4,256,384]{1,2,0:T(8,128)(2,1)} %copy.118), channel_id=1, replica_groups=mesh['sp'=32,'tp'=4] {'tp'}, dimensions={0} | all-to-all | bytes 1572864 | tf_op jit(solution)/shard_map/all_to_all | solution.py:283
  371.6 3.5 fusion.178
  375.1 1.7 fusion.76
  (422 shorter events, 128.8 us)
Async XLA Ops:
  6.5 368.6 %copy-start = (bf16[512,2048]{1,0:T(8,128)(2,1)S(1)}, bf16[512,2048]{1,0:T(8,128)(2,1)}, u32[]{:S(2)}) copy-start(bf16[512,2048]{1,0:T(8,128)(2,1)} %param.42) | copy-start | bytes 6291460
  6.5 7.1 %copy-start.8 = (bf16[2048,256]{1,0:T(8,128)(2,1)S(1)}, bf16[2048,256]{1,0:T(8,128)(2,1)}, u32[]{:S(2)}) copy-start(bf16[2048,256]{1,0:T(8,128)(2,1)} %param.28) | copy-start | bytes 3145732
  6.5 53.7 %all-gather.9.cloned.1.call-start = ((), (), s32[]{:S(2)}) async-start(), calls=%async_computation.1 | async-start | bytes 5242880 | tf_op jit(solution)/shard_map/all_gather | solution.py:186
  7.3 322.2 %all-gather.11.cloned.1.call-start = ((), (), s32[]{:S(2)}) async-start(), calls=%async_computation.2 | async-start | bytes 4325376 | tf_op jit(solution)/shard_map/all_gather | solution.py:257
  8.4 6.2 %copy-start.9 = (bf16[2048,256]{1,0:T(8,128)(2,1)S(1)}, bf16[2048,256]{1,0:T(8,128)(2,1)}, u32[]{:S(2)}) copy-start(bf16[2048,256]{1,0:T(8,128)(2,1)} %param.29) | copy-start | bytes 3145732
  8.5 7.3 %copy-start.10 = (bf16[2048,256]{1,0:T(8,128)(2,1)S(1)}, bf16[2048,256]{1,0:T(8,128)(2,1)}, u32[]{:S(2)}) copy-start(bf16[2048,256]{1,0:T(8,128)(2,1)} %param.30) | copy-start | bytes 3145732
  14.7 49.2 %copy-start.21 = (f32[2048]{0:T(1024)S(1)}, f32[2048]{0:T(1024)}, u32[]{:S(2)}) copy-start(f32[2048]{0:T(1024)} %param.25) | copy-start | bytes 24580
  60.2 3.6 copy-start.5
  72.4 3.5 copy-start.7
  73.9 0.8 copy-start.1
  75.9 8.8 %copy-start.3 = (bf16[2,1024,128]{2,1,0:T(8,128)(2,1)}, bf16[2,1024,128]{2,1,0:T(8,128)(2,1)S(1)}, u32[]{:S(2)}) copy-start(bf16[2,1024,128]{2,1,0:T(8,128)(2,1)S(1)} %get-tuple-element.407) | copy-start | bytes 1572868
  81.0 3.7 copy-start.12
  81.0 3.7 copy-start.13
  172.9 113.0 %copy-start.15 = (f32[2,2]{1,0:T(2,128)S(1)}, f32[2,2]{1,0:T(2,128)}, u32[]{:S(2)}) copy-start(f32[2,2]{1,0:T(2,128)} %param.38) | copy-start | bytes 52
  172.9 142.5 %copy-start.14 = (f32[2,2,128]{2,1,0:T(2,128)S(1)}, f32[2,2,128]{2,1,0:T(2,128)}, u32[]{:S(2)}) copy-start(f32[2,2,128]{2,1,0:T(2,128)} %param.37) | copy-start | bytes 6148
  231.0 92.6 %copy-start.6 = (f32[8,2,128,128]{3,2,1,0:T(8,128)S(1)}, f32[8,2,128,128]{3,2,1,0:T(8,128)}, u32[]{:S(2)}) copy-start(f32[8,2,128,128]{3,2,1,0:T(8,128)} %get-tuple-element.142) | copy-start | bytes 3145732
  286.8 40.5 %collective-permute-start.1 = (bf16[8,128]{1,0:T(8,128)(2,1)S(1)}, bf16[8,128]{1,0:T(8,128)(2,1)S(1)}, u32[]{:S(2)}, u32[]{:S(2)}) collective-permute-start(bf16[8,128]{1,0:T(8,128)(2,1)S(1)} %get-tuple-element.374), channel_id=1, source_target_pairs={{4,0},{8,4},{12,8},{16,12},{20,16},{24,20},{28,24},{32,28},{36,32}... | collective-permute-start | bytes 6152 | tf_op jit(solution)/shard_map/ppermute | solution.py:24
  288.9 38.4 %collective-permute-start = (bf16[8,128]{1,0:T(8,128)(2,1)S(1)}, bf16[8,128]{1,0:T(8,128)(2,1)S(1)}, u32[]{:S(2)}, u32[]{:S(2)}) collective-permute-start(bf16[8,128]{1,0:T(8,128)(2,1)S(1)} %get-tuple-element.373), channel_id=1, source_target_pairs={{0,4},{4,8},{8,12},{12,16},{16,20},{20,24},{24,28},{28,32},{32,36}... | collective-permute-start | bytes 6152 | tf_op jit(solution)/shard_map/ppermute | solution.py:21
  315.1 1.9 copy-start.16
  315.1 0.5 copy-start.18
  318.4 8.9 %slice-start = ((bf16[1024,1152]{1,0:T(8,128)(2,1)}), bf16[1024,128]{1,0:T(8,128)(2,1)S(1)}, s32[]{:S(2)}) async-start(bf16[1024,1152]{1,0:T(8,128)(2,1)} %copy-done.7), calls=%async_computation.3 | async-start | bytes 524288 | tf_op jit(solution)/shard_map/slice | solution.py:195
  318.4 8.9 %copy-start.22 = (f32[128]{0:T(128)S(1)}, f32[128]{0:T(128)}, u32[]{:S(2)}) copy-start(f32[128]{0:T(128)} %dynamic_slice.60) | copy-start | bytes 1540
  329.5 5.5 %copy-start.4 = (bf16[2,1024,128]{2,1,0:T(8,128)(2,1)S(1)}, bf16[2,1024,128]{2,1,0:T(8,128)(2,1)}, u32[]{:S(2)}) copy-start(bf16[2,1024,128]{2,1,0:T(8,128)(2,1)} %rev.22) | copy-start | bytes 1572868
  329.5 5.5 %copy-start.11 = (f32[2,1024,128]{1,2,0:T(8,128)S(1)}, f32[2,1024,128]{1,2,0:T(8,128)}, u32[]{:S(2)}) copy-start(f32[2,1024,128]{1,2,0:T(8,128)} %reshape.649) | copy-start | bytes 3145732
  329.5 5.5 %copy-start.19 = (f32[2]{0:T(128)S(1)}, f32[2]{0:T(128)}, u32[]{:S(2)}) copy-start(f32[2]{0:T(128)} %copy-done.18) | copy-start | bytes 28
  329.5 5.5 %copy-start.20 = (f32[2,2,128,128]{3,2,1,0:T(8,128)S(1)}, f32[2,2,128,128]{3,2,1,0:T(8,128)}, u32[]{:S(2)}) copy-start(f32[2,2,128,128]{3,2,1,0:T(8,128)} %param.36) | copy-start | bytes 786436
  335.0 13.6 %copy-start.2 = (bf16[128,2,8,128]{3,2,1,0:T(8,128)(2,1)S(1)}, bf16[128,2,8,128]{3,2,1,0:T(8,128)(2,1)}, u32[]{:S(2)}) copy-start(bf16[128,2,8,128]{3,2,1,0:T(8,128)(2,1)} %copy-done.1) | copy-start | bytes 1572868
  335.0 13.6 %copy-start.17 = (f32[2]{0:T(128)S(1)}, f32[2]{0:T(128)}, u32[]{:S(2)}) copy-start(f32[2]{0:T(128)} %copy-done.16) | copy-start | bytes 28
Sparse Core Ops, SparseCore 0:
  9.0 51.1 all-gather.8
  231.8 47.1 all-gather.10
where the time goes:
time: 390 us; the launch traced here: 384 us
  matrix products  134 us (34%)
  blocking collectives  86.9 us (22%)
  local copies, waits for them, and re-layouts  71.2 us (18%)
  waiting for transfers between devices  44.1 us (11%)
  other arithmetic  26.8 us (7%)
  between operations  14 us (4%)
  starting transfers between devices  5.59 us (1%)
    all_gather x3, blocking collectives, per_device(): gathered = lax.all_gather(stacked, 'sp', axis=0, tiled=True)  71.4 us
    all_gather x1, waiting for transfers between devices, per_device(): whole_rows = lax.all_gather(tokens, 'tp', axis=1, tiled=True)  43.3 us
    dot_general x16, matrix products, block_step(): jnp.einsum('hts,hsv->htv', scores, v_blk)  21.4 us
    dot_general x16, matrix products, block_step(): jnp.einsum('hsv,hsk->hvk', v_blk * weights[:, :, None], k_blk)  18.7 us
    dot_general x16, matrix products, block_step(): jnp.einsum('htd,hsd->hts', q_blk, k_blk)  16.9 us
    dot_general x16, matrix products, block_step(): jnp.einsum('hvk,htk->htv', memory, q_blk)  16.6 us
    dot_general x16, matrix products, block_step(): jnp.einsum('hk,htk->ht', normer, q_blk)  15.5 us
    all_to_all x1, blocking collectives, per_device(): owned = lax.all_to_all(mixed, 'tp', split_axis=0, concat_axis=1, tiled=True)  15.5 us
  transfers between devices with their start and end apart: 4, of which 1 were waited for; matrix products, arithmetic and copies ran while one was open for 8% of the time, Pallas kernels for 0%

commit v1 on v0

v1 whole, which is shorter than its diff:
```python
import functools
import math

import jax
import jax.numpy as jnp
from jax import lax
from jax.experimental import pallas as pl
from jax.experimental.pallas import tpu as pltpu
from jax.sharding import PartitionSpec as P

DH = 128
EXT = 144
TP = 4
MARGIN = 64
RIM = 16
NEG_BIG = -1e30
LN_EPS = 1e-05
HEAD_EPS = 1e-06
MESH = pl.DeviceIdType.MESH
F32 = jnp.float32
BF16 = jnp.bfloat16
TRANS_B = (((1,), (1,)), ((), ()))


def dot(a, b):
    return jnp.dot(a, b, preferred_element_type=F32)


def dot_t(a, b):
    return lax.dot_general(a, b, TRANS_B, preferred_element_type=F32)


def combine(items):
    after = None
    logs = []
    for fall, top in reversed(items):
        logs.append(top if after is None else top + after)
        after = fall if after is None else after + fall
    logs.reverse()
    joint = functools.reduce(jnp.maximum, logs)
    return [jnp.exp(one - joint) for one in logs], after, joint


def kernel(
    ny,
    nz,
    tok,
    gain,
    wp_hbm,
    wq_hbm,
    wk_hbm,
    wv_hbm,
    wo_hbm,
    gin,
    gfg,
    bias,
    fscale,
    fextra,
    start_c,
    start_n,
    start_m,
    gmap,
    pscale,
    hgain,
    wpo_hbm,
    wmo_hbm,
    out,
    xg,
    wp,
    wq,
    wk,
    wv,
    wo,
    wpo,
    wmo,
    nb,
    qs,
    ks,
    vt,
    og,
    pool,
    gt,
    gsc,
    tri,
    xl,
    ar,
    cst,
    bs,
    ms,
    sum_c,
    sum_s,
    r0_c,
    r0_s,
    y_c,
    y_s,
    z_c,
    z_s,
    p_c,
    p_s,
    r3_c,
    r3_s,
    ent_c,
    ent_m,
    est,
    em,
    psend,
    pbuf,
    msend,
    mbuf,
    acc,
    load_sem,
    own_ss,
    own_rs,
    fwd_ss,
    fwd_rs,
    r0_ss,
    r0_rs,
    y_ss,
    y_rs,
    z_ss,
    z_rs,
    r3_ss,
    r3_rs,
    halo_ss,
    halo_rs,
    pool_ss,
    pool_rs,
    mem_ss,
    mem_rs,
):
    rows = tok.shape[0]
    width = tok.shape[1]
    ch = rows // TP
    hf = ch // 2
    t = lax.axis_index("tp")
    s = lax.axis_index("sp")
    ns = 2 * ny * nz
    core = lax.rem(s, 2)
    yi = lax.rem(s // 2, ny)
    zi = s // (2 * ny)
    partner = s + 1 - 2 * core
    right = lax.rem(t + 1, TP)
    left = lax.rem(t + 3, TP)
    step = 1 - 2 * core
    half_log = F32(0) + (-0.5 * math.log(DH))

    loads = []
    for index, (src, dst) in enumerate(
        (
            (wq_hbm, wq),
            (wk_hbm, wk),
            (wv_hbm, wv),
            (wo_hbm, wo),
            (wp_hbm, wp),
            (wpo_hbm, wpo),
            (wmo_hbm, wmo),
            (tok, xg.at[t]),
        )
    ):
        loads.append(pltpu.make_async_copy(src, dst, load_sem.at[index]))
    loads[7].start()

    barrier = pltpu.get_barrier_semaphore()
    peers = [(s, lax.rem(t + j, TP)) for j in range(1, TP)]
    peers.append((partner, t))
    peers += [((zi * ny + lax.rem(yi + j, ny)) * 2 + core, t) for j in range(1, ny)]
    peers += [((lax.rem(zi + j, nz) * ny + yi) * 2 + core, t) for j in range(1, nz)]
    peers += [(lax.rem(s + 1, ns), t), (lax.rem(s + ns - 1, ns), t)]
    pool[0:MARGIN] = jnp.zeros((MARGIN, DH), BF16)
    pool[MARGIN + rows : 2 * MARGIN + rows] = jnp.zeros((MARGIN, DH), BF16)
    z_c[...] = jnp.zeros_like(z_c)
    z_s[...] = jnp.zeros_like(z_s)
    for peer in peers:
        pl.semaphore_signal(barrier, inc=1, device_id=peer, device_id_type=MESH)
    pl.semaphore_wait(barrier, len(peers))

    def own_copy(c, way):
        span = pl.ds(pl.multiple_of(c * ch, ch), ch)
        return pltpu.make_async_remote_copy(
            src_ref=tok.at[span],
            dst_ref=xg.at[t, span],
            send_sem=own_ss.at[way, c],
            recv_sem=own_rs.at[way, c],
            device_id=(s, right if way == 0 else left),
            device_id_type=MESH,
        )

    def fwd_copy(c, way):
        span = pl.ds(pl.multiple_of(c * ch + way * hf, hf), hf)
        slot = left if way == 0 else right
        return pltpu.make_async_remote_copy(
            src_ref=xg.at[slot, span],
            dst_ref=xg.at[slot, span],
            send_sem=fwd_ss.at[way, c],
            recv_sem=fwd_rs.at[way, c],
            device_id=(s, right if way == 0 else left),
            device_id_type=MESH,
        )

    for c in (0, 1):
        for way in (0, 1):
            own_copy(c, way).start()
    for one in loads[:7]:
        one.start()

    gt[...] = jnp.concatenate(
        [gin[0].astype(F32), gin[1].astype(F32), gfg[0].astype(F32), gfg[1].astype(F32)], axis=0
    ).astype(BF16)
    row_of = lax.broadcasted_iota(jnp.int32, (ch, ch), 0)
    col_of = lax.broadcasted_iota(jnp.int32, (ch, ch), 1)
    tri[:, 0:ch] = jnp.where(row_of <= col_of, 1.0, 0.0).astype(BF16)
    tri[:, ch : 2 * ch] = jnp.where(row_of >= col_of, 1.0, 0.0).astype(BF16)
    tail = lax.broadcasted_iota(jnp.int32, (EXT - DH, rows), 0)
    ones_row = jnp.where(tail == 0, 1.0, 0.0).astype(BF16)
    for h in range(2):
        vt[h, DH:EXT, :] = ones_row

    loads[7].wait()
    for way in (0, 1):
        own_copy(0, way).wait_recv()
        fwd_copy(0, way).start()
        own_copy(2, way).start()
    for one in loads[:5]:
        one.wait()

    def chunk(c, carry):
        @pl.when(c + 1 < TP)
        def _():
            for way in (0, 1):
                own_copy(c + 1, way).wait_recv()
                fwd_copy(c + 1, way).start()

        @pl.when(c + 3 < TP)
        def _():
            for way in (0, 1):
                own_copy(c + 3, way).start()

        for way in (0, 1):
            slot = left if way == 0 else right
            span = pl.ds(pl.multiple_of(c * ch + way * hf, hf), hf)
            far = lax.rem(t + 2, TP)
            pltpu.make_async_remote_copy(
                src_ref=xg.at[far, span],
                dst_ref=xg.at[far, span],
                send_sem=fwd_ss.at[way, c],
                recv_sem=fwd_rs.at[way, c],
                device_id=(s, slot),
                device_id_type=MESH,
            ).wait_recv()

        base = pl.multiple_of(c * ch, ch)
        span = pl.ds(base, ch)
        sub = 64

        def norm(i, carry):
            at = pl.multiple_of(i * sub, sub)
            inner = pl.ds(pl.multiple_of(base + at, sub), sub)
            total = jnp.zeros((sub, DH), F32)
            squares = jnp.zeros((sub, DH), F32)
            for j in range(TP):
                for l in range(width // DH):
                    x = xg[j, inner, l * DH : (l + 1) * DH].astype(F32)
                    total = total + x
                    squares = squares + x * x
            mean = jnp.sum(total, axis=1, keepdims=True) / (TP * width)
            var = jnp.sum(squares, axis=1, keepdims=True) / (TP * width) - mean * mean
            scale = lax.rsqrt(var + LN_EPS)
            mean = jnp.broadcast_to(mean, (sub, DH))
            scale = jnp.broadcast_to(scale, (sub, DH))
            for j in range(TP):
                for l in range(width // DH):
                    x = xg[j, inner, l * DH : (l + 1) * DH].astype(F32)
                    f = j * width + l * DH
                    nb[pl.ds(at, sub), f : f + DH] = (
                        (x - mean) * scale * gain[0:1, f : f + DH]
                    ).astype(BF16)
            return carry

        lax.fori_loop(0, ch // sub, norm, 0)
        normed = nb[...]
        gsc[...] = dot_t(gt[...], normed)
        k_all = dot(normed, wk[...]).astype(BF16)
        q_all = dot(normed, wq[...]).astype(BF16)
        v_all = dot(normed, wv[...]).astype(BF16).astype(F32).T.astype(BF16)
        ks[span] = k_all
        qs[span] = q_all
        og[span] = dot(normed, wo[...]).astype(BF16)
        pool[pl.ds(pl.multiple_of(base + MARGIN, MARGIN), ch)] = dot(normed, wp[...]).astype(BF16)
        for h in range(2):
            vt[h, 0:DH, span] = v_all[h * DH : (h + 1) * DH]

        ins = []
        fgs = []
        for r in range(2):
            for h in range(2):
                ins.append(gsc[pl.ds(8 * r + 2 * t + h, 1), :])
                x = gsc[pl.ds(16 + 8 * r + 2 * t + h, 1), :] + bias[r, 2 * t + h]
                fgs.append(
                    (jnp.minimum(x, 0.0) - jnp.log1p(jnp.exp(-jnp.abs(x)))) * fscale[r : r + 1, span]
                    + fextra[r : r + 1, span]
                )
        blank = jnp.zeros((4, ch), F32)
        log_in = jnp.concatenate(ins + [blank], axis=0)
        log_fg = jnp.concatenate(fgs + [blank], axis=0)
        high = log_fg.astype(BF16).astype(F32)
        rest = log_fg - high
        mid = rest.astype(BF16).astype(F32)
        low = rest - mid
        parts = jnp.concatenate([high, mid, low, jnp.zeros((8, ch), F32)], axis=0).astype(BF16)
        sums = dot(parts, tri[...])
        sums = sums[0:8] + sums[8:16] + sums[16:24]
        which = lax.broadcasted_iota(jnp.int32, (8, ch), 0)
        falls = jnp.where(which < 2, sums[:, 0:ch], sums[:, ch : 2 * ch])
        a_row = log_in - falls
        a_col = jnp.concatenate([a_row, jnp.zeros((DH - 8, ch), F32)], axis=0).T
        peak = jnp.max(a_row, axis=1, keepdims=True)
        weight = jnp.exp(a_row - peak + half_log)
        ends = jnp.where(which[:, 0:1] < 2, falls[:, ch - 1 : ch], falls[:, 0:1])
        bs[c] = jnp.broadcast_to(ends, (8, DH))
        ms[c] = jnp.broadcast_to(ends + peak, (8, DH))
        rr = lax.broadcasted_iota(jnp.int32, (ch, ch), 0)
        cc = lax.broadcasted_iota(jnp.int32, (ch, ch), 1)
        for h in range(2):
            k_h = k_all[:, h * DH : (h + 1) * DH]
            q_h = q_all[:, h * DH : (h + 1) * DH]
            scores = dot_t(k_h, q_h)
            v_ext = vt[h, :, span]
            for r in range(2):
                ci = 2 * r + h
                inside = (rr <= cc) if r == 0 else (rr >= cc)
                expo = jnp.where(inside, a_col[:, ci : ci + 1], NEG_BIG)
                top = jnp.max(expo, axis=0, keepdims=True)
                probs = (scores * jnp.exp(expo - top + half_log)).astype(BF16)
                xl[ci, :, span] = dot(v_ext, probs)
                ar[pl.ds(ci, 1), span] = top
                cst[c, ci] = dot((v_ext.astype(F32) * weight[ci : ci + 1]).astype(BF16), k_h)
        return carry

    lax.fori_loop(0, TP, chunk, 0)

    to_prev = pltpu.make_async_remote_copy(
        src_ref=pool.at[pl.ds(MARGIN, RIM)],
        dst_ref=pool.at[pl.ds(MARGIN + rows, RIM)],
        send_sem=halo_ss.at[0],
        recv_sem=halo_rs.at[0],
        device_id=(lax.rem(s + ns - 1, ns), t),
        device_id_type=MESH,
    )
    to_next = pltpu.make_async_remote_copy(
        src_ref=pool.at[pl.ds(MARGIN + rows - RIM, RIM)],
        dst_ref=pool.at[pl.ds(MARGIN - RIM, RIM)],
        send_sem=halo_ss.at[1],
        recv_sem=halo_rs.at[1],
        device_id=(lax.rem(s + 1, ns), t),
        device_id_type=MESH,
    )

    for r in range(2):
        order = list(range(TP)) if r == 0 else list(range(TP - 1, -1, -1))
        for h in range(2):
            ci = 2 * r + h
            weights, fall, top = combine(
                [(bs[b, ci : ci + 1, :], ms[b, ci : ci + 1, :]) for b in order]
            )
            total = None
            for b, w in zip(order, weights):
                term = w * cst[b, ci]
                total = term if total is None else total + term
            sum_c[r, h] = total.astype(BF16)
            sum_s[r, h : h + 1, :] = fall
            sum_s[r, 2 + h : 3 + h, :] = top

    def pair(src_c, src_s, dst_c, dst_s, ss, rs, who):
        return [
            pltpu.make_async_remote_copy(
                src_ref=a, dst_ref=b, send_sem=ss.at[i], recv_sem=rs.at[i], device_id=who, device_id_type=MESH
            )
            for i, (a, b) in enumerate(((src_c, dst_c), (src_s, dst_s)))
        ]

    swap = pair(sum_c.at[1 - core], sum_s.at[1 - core], r0_c, r0_s, r0_ss, r0_rs, (partner, t))
    for one in swap:
        one.start()

    @pl.when(s > 0)
    def _():
        to_prev.start()

    @pl.when(s < ns - 1)
    def _():
        to_next.start()

    for one in swap:
        one.wait_recv()
    for h in range(2):
        weights, fall, top = combine(
            [
                (sum_s[core, h : h + 1, :], sum_s[core, 2 + h : 3 + h, :]),
                (r0_s[h : h + 1, :], r0_s[2 + h : 3 + h, :]),
            ]
        )
        y_c[yi, h] = (
            weights[0] * sum_c[core, h].astype(F32) + weights[1] * r0_c[h].astype(F32)
        ).astype(BF16)
        y_s[yi, h : h + 1, :] = fall
        y_s[yi, 2 + h : 3 + h, :] = top

    def y_pair(j, slot):
        who = ((zi * ny + lax.rem(yi + j, ny)) * 2 + core, t)
        return pair(
            y_c.at[slot], y_s.at[slot], y_c.at[slot], y_s.at[slot], y_ss.at[j], y_rs.at[slot], who
        )

    for j in range(1, ny):
        for one in y_pair(j, yi):
            one.start()

    @pl.when(s < ns - 1)
    def _():
        to_prev.wait_recv()

    @pl.when(s > 0)
    def _():
        to_next.wait_recv()

    half_span = jnp.left_shift(jnp.int32(1), t)
    map_own = gmap[t]
    scale_own = pscale[0:1, pl.ds(pl.multiple_of(t * DH, DH), DH)]

    def pool_copy(blk, off):
        return pltpu.make_async_remote_copy(
            src_ref=psend.at[blk],
            dst_ref=pbuf.at[t],
            send_sem=pool_ss.at[off],
            recv_sem=pool_rs.at[t],
            device_id=(s, blk),
            device_id_type=MESH,
        )

    ext = ch + 2 * MARGIN
    at_row = lax.broadcasted_iota(jnp.int32, (ch, ext), 0)
    at_col = lax.broadcasted_iota(jnp.int32, (ch, ext), 1) - MARGIN
    band = jnp.where((at_col >= at_row - half_span) & (at_col < at_row + half_span), 1.0, 0.0)
    band = band.astype(BF16)

    def pool_block(i, carry):
        off = jnp.where(i == 0, 2, jnp.where(i == 1, 1, jnp.where(i == 2, 3, 0)))
        blk = lax.rem(t + off, TP)
        base = pl.multiple_of(blk * ch, ch)
        near = pool[pl.ds(base, ext), :]
        pooled = dot(band, near)
        pos = s * rows + base + lax.broadcasted_iota(jnp.int32, (ch, 1), 0)
        counts = jnp.minimum(pos + half_span, ns * rows) - jnp.maximum(pos - half_span, 0)
        own = near[MARGIN : MARGIN + ch].astype(F32)
        contrast = (pooled / counts.astype(F32) - own).astype(BF16)
        result = (dot(contrast, map_own) * scale_own).astype(BF16)

        @pl.when(i < 3)
        def _():
            psend[blk] = result
            pool_copy(blk, off).start()

        @pl.when(i == 3)
        def _():
            pbuf[blk] = result

        return carry

    lax.fori_loop(0, TP, pool_block, 0)

    for j in range(1, ny):
        for one in y_pair(j, lax.rem(yi + j, ny)):
            one.wait_recv()
    y_slots = [core * (ny - 1) + i * step for i in range(ny)]
    for h in range(2):
        weights, fall, top = combine(
            [(y_s[i, h : h + 1, :], y_s[i, 2 + h : 3 + h, :]) for i in y_slots]
        )
        total = None
        for i, w in zip(y_slots, weights):
            term = w * y_c[i, h].astype(F32)
            total = term if total is None else total + term
        z_c[zi, h] = total.astype(BF16)
        z_s[zi, h : h + 1, :] = fall
        z_s[zi, 2 + h : 3 + h, :] = top

    def z_pair(j, slot):
        to = zi + j * step
        who = ((to * ny + yi) * 2 + core, t)
        return pair(
            z_c.at[slot], z_s.at[slot], z_c.at[slot], z_s.at[slot], z_ss.at[j], z_rs.at[slot], who
        )

    for j in range(1, nz):

        @pl.when((zi + j * step >= 0) & (zi + j * step < nz))
        def _():
            for one in z_pair(j, zi):
                one.start()

    for one in loads[5:7]:
        one.wait()
    for j in range(1, TP):
        src = lax.rem(t + j, TP)
        pltpu.make_async_remote_copy(
            src_ref=psend.at[src],
            dst_ref=pbuf.at[src],
            send_sem=pool_ss.at[j],
            recv_sem=pool_rs.at[src],
            device_id=(s, src),
            device_id_type=MESH,
        ).wait_recv()
    cols = 512

    def pool_out(i, carry):
        span = pl.ds(pl.multiple_of(i * cols, cols), cols)
        total = None
        for j in range(TP):
            term = dot(pbuf[j], wpo[j * DH : (j + 1) * DH, span])
            total = term if total is None else total + term
        acc[:, span] = total
        return carry

    lax.fori_loop(0, acc.shape[1] // cols, pool_out, 0)

    for j in range(1, nz):
        src = zi - j * step

        @pl.when((src >= 0) & (src < nz))
        def _():
            who = ((src * ny + yi) * 2 + core, t)
            for one in pair(
                z_c.at[src], z_s.at[src], z_c.at[src], z_s.at[src], z_ss.at[j], z_rs.at[src], who
            ):
                one.wait_recv()

    y_rel = jnp.where(core == 0, yi, ny - 1 - yi)
    z_rel = jnp.where(core == 0, zi, nz - 1 - zi)
    z_slots = [core * (nz - 1) + i * step for i in range(nz - 1)]
    for h in range(2):
        items = [(jnp.zeros((1, DH), F32), jnp.full((1, DH), start_m[core, h], F32))]
        for i, slot in enumerate(z_slots):
            valid = i < z_rel
            items.append(
                (
                    jnp.where(valid, z_s[slot, h : h + 1, :], 0.0),
                    jnp.where(valid, z_s[slot, 2 + h : 3 + h, :], NEG_BIG),
                )
            )
        for i, slot in enumerate(y_slots[: ny - 1]):
            valid = i < y_rel
            items.append(
                (
                    jnp.where(valid, y_s[slot, h : h + 1, :], 0.0),
                    jnp.where(valid, y_s[slot, 2 + h : 3 + h, :], NEG_BIG),
                )
            )
        weights, fall, top = combine(items)
        total = None
        for slot, w in zip(z_slots, weights[1 : 1 + len(z_slots)]):
            term = w * z_c[slot, h].astype(F32)
            total = term if total is None else total + term
        for slot, w in zip(y_slots[: ny - 1], weights[1 + len(z_slots) :]):
            term = w * y_c[slot, h].astype(F32)
            total = term if total is None else total + term
        ent_c[core, h] = total
        ent_c[core, h, 0:DH, :] += weights[0] * start_c[core, h]
        ent_c[core, h, DH : DH + 1, :] += weights[0] * start_n[core, h : h + 1, :]
        ent_m[core, h : h + 1, :] = top
        weights, fall, later = combine(
            [
                (jnp.zeros((1, DH), F32), top),
                (sum_s[core, h : h + 1, :], sum_s[core, 2 + h : 3 + h, :]),
            ]
        )
        p_c[h] = (weights[0] * ent_c[core, h] + weights[1] * sum_c[core, h].astype(F32)).astype(BF16)
        p_s[h : h + 1, :] = later
    give = pair(p_c, p_s, r3_c, r3_s, r3_ss, r3_rs, (partner, t))
    for one in give:
        one.start()
    for one in give:
        one.wait_recv()
    for h in range(2):
        ent_c[1 - core, h] = r3_c[h].astype(F32)
        ent_m[1 - core, h : h + 1, :] = r3_s[h : h + 1, :]

    for r in range(2):
        order = list(range(TP)) if r == 0 else list(range(TP - 1, -1, -1))
        for h in range(2):
            ci = 2 * r + h
            state = ent_c[r, h]
            top = ent_m[r, h : h + 1, :]
            for at, b in enumerate(order):
                est[b, ci] = state.astype(BF16)
                em[b, ci : ci + 1, :] = top
                if at < TP - 1:
                    weights, fall, later = combine(
                        [
                            (top, top),
                            (bs[b, ci : ci + 1, :], ms[b, ci : ci + 1, :]),
                        ]
                    )
                    state = weights[0] * state + weights[1] * cst[b, ci]
                    top = later

    def mem_copy(blk, off):
        return pltpu.make_async_remote_copy(
            src_ref=msend.at[blk],
            dst_ref=mbuf.at[t],
            send_sem=mem_ss.at[off],
            recv_sem=mem_rs.at[t],
            device_id=(s, blk),
            device_id_type=MESH,
        )

    def finish(i, carry):
        off = jnp.where(i == 0, 2, jnp.where(i == 1, 1, jnp.where(i == 2, 3, 0)))
        blk = lax.rem(t + off, TP)
        span = pl.ds(pl.multiple_of(blk * ch, ch), ch)
        pieces = []
        for h in range(2):
            q_h = qs[span, h * DH : (h + 1) * DH]
            hidden = None
            for r in range(2):
                ci = 2 * r + h
                from_state = dot_t(est[blk, ci], q_h)
                local_top = ar[pl.ds(ci, 1), span]
                state_top = em[blk, ci : ci + 1, 0:1]
                joint = jnp.maximum(local_top, state_top)
                local_w = jnp.exp(local_top - joint)
                state_w = jnp.exp(state_top - joint)
                den = (
                    local_w * xl[ci, DH : DH + 1, span] + state_w * from_state[DH : DH + 1]
                )
                inverse = 1.0 / jnp.maximum(jnp.abs(den), 1.0)
                term = (local_w * inverse) * xl[ci, 0:DH, span] + (state_w * inverse) * from_state[0:DH]
                hidden = term if hidden is None else hidden + term
            mean = jnp.mean(hidden, axis=0, keepdims=True)
            centred = hidden - mean
            var = jnp.mean(centred * centred, axis=0, keepdims=True)
            scaled = (centred * lax.rsqrt(var + HEAD_EPS)).T
            g_at = pl.multiple_of(t * 2 * DH + h * DH, DH)
            gate = jax.nn.sigmoid(og[span, h * DH : (h + 1) * DH].astype(F32))
            pieces.append((scaled * hgain[0:1, pl.ds(g_at, DH)] * gate).astype(BF16))

        @pl.when(i < 3)
        def _():
            for h in range(2):
                msend[blk, :, h * DH : (h + 1) * DH] = pieces[h]
            mem_copy(blk, off).start()

        @pl.when(i == 3)
        def _():
            for h in range(2):
                mbuf[blk, :, h * DH : (h + 1) * DH] = pieces[h]

        return carry

    lax.fori_loop(0, TP, finish, 0)

    def mem_part(src, last):
        def body(i, carry):
            span = pl.ds(pl.multiple_of(i * cols, cols), cols)
            at = pl.multiple_of(src * 2 * DH, 2 * DH)
            total = acc[:, span] + dot(mbuf[src], wmo[pl.ds(at, 2 * DH), span])
            if last:
                out[:, span] = total.astype(BF16)
            else:
                acc[:, span] = total
            return carry

        lax.fori_loop(0, acc.shape[1] // cols, body, 0)

    mem_part(t, False)
    for j in (1, 3, 2):
        src = lax.rem(t + j, TP)
        pltpu.make_async_remote_copy(
            src_ref=msend.at[src],
            dst_ref=mbuf.at[src],
            send_sem=mem_ss.at[j],
            recv_sem=mem_rs.at[src],
            device_id=(s, src),
            device_id_type=MESH,
        ).wait_recv()
        mem_part(src, j == 2)

    for c in range(TP):
        for way in (0, 1):
            own_copy(c, way).wait_send()
            fwd_copy(c, way).wait_send()
    for one in swap + give:
        one.wait_send()

    @pl.when(s > 0)
    def _():
        to_prev.wait_send()

    @pl.when(s < ns - 1)
    def _():
        to_next.wait_send()

    for j in range(1, ny):
        for one in y_pair(j, yi):
            one.wait_send()
    for j in range(1, nz):

        @pl.when((zi + j * step >= 0) & (zi + j * step < nz))
        def _():
            for one in z_pair(j, zi):
                one.wait_send()

    for j in range(1, TP):
        blk = lax.rem(t + j, TP)
        pool_copy(blk, j).wait_send()
        mem_copy(blk, j).wait_send()


def per_device(ny, nz, *args):
    (
        tokens,
        input_norm_gain,
        pooling_input_matrix,
        query_projection_matrix,
        key_projection_matrix,
        value_projection_matrix,
        output_gate_matrix,
        input_gate_matrix,
        forget_gate_matrix,
        forget_gate_bias,
        log_forget_scale,
        extra_log_forget,
        starting_memory,
        starting_normalizer,
        starting_log_scale,
        pooling_group_map,
        pooling_channel_scale,
        memory_head_gain,
        pooling_output_matrix,
        memory_output_matrix,
    ) = args
    rows, width = tokens.shape
    model = width * TP
    ch = rows // TP
    vmem = pl.BlockSpec(memory_space=pltpu.VMEM)
    smem = pl.BlockSpec(memory_space=pltpu.SMEM)
    hbm = pl.BlockSpec(memory_space=pl.ANY)
    dma = pltpu.SemaphoreType.DMA
    scratch = [
        pltpu.VMEM((TP, rows, width), BF16),
        pltpu.VMEM((model, DH), BF16),
        pltpu.VMEM((model, 2 * DH), BF16),
        pltpu.VMEM((model, 2 * DH), BF16),
        pltpu.VMEM((model, 2 * DH), BF16),
        pltpu.VMEM((model, 2 * DH), BF16),
        pltpu.VMEM(pooling_output_matrix.shape, BF16),
        pltpu.VMEM(memory_output_matrix.shape, BF16),
        pltpu.VMEM((ch, model), BF16),
        pltpu.VMEM((rows, 2 * DH), BF16),
        pltpu.VMEM((rows, 2 * DH), BF16),
        pltpu.VMEM((2, EXT, rows), BF16),
        pltpu.VMEM((rows, 2 * DH), BF16),
        pltpu.VMEM((rows + 2 * MARGIN, DH), BF16),
        pltpu.VMEM((32, model), BF16),
        pltpu.VMEM((32, ch), F32),
        pltpu.VMEM((ch, 2 * ch), BF16),
        pltpu.VMEM((4, EXT, rows), F32),
        pltpu.VMEM((8, rows), F32),
        pltpu.VMEM((TP, 4, EXT, DH), F32),
        pltpu.VMEM((TP, 8, DH), F32),
        pltpu.VMEM((TP, 8, DH), F32),
        pltpu.VMEM((2, 2, EXT, DH), BF16),
        pltpu.VMEM((2, 8, DH), F32),
        pltpu.VMEM((2, EXT, DH), BF16),
        pltpu.VMEM((8, DH), F32),
        pltpu.VMEM((ny, 2, EXT, DH), BF16),
        pltpu.VMEM((ny, 8, DH), F32),
        pltpu.VMEM((nz, 2, EXT, DH), BF16),
        pltpu.VMEM((nz, 8, DH), F32),
        pltpu.VMEM((2, EXT, DH), BF16),
        pltpu.VMEM((8, DH), F32),
        pltpu.VMEM((2, EXT, DH), BF16),
        pltpu.VMEM((8, DH), F32),
        pltpu.VMEM((2, 2, EXT, DH), F32),
        pltpu.VMEM((2, 8, DH), F32),
        pltpu.VMEM((TP, 4, EXT, DH), BF16),
        pltpu.VMEM((TP, 8, DH), F32),
        pltpu.VMEM((TP, ch, DH), BF16),
        pltpu.VMEM((TP, ch, DH), BF16),
        pltpu.VMEM((TP, ch, 2 * DH), BF16),
        pltpu.VMEM((TP, ch, 2 * DH), BF16),
        pltpu.VMEM((ch, model), F32),
        dma((8,)),
        dma((2, TP)),
        dma((2, TP)),
        dma((2, TP)),
        dma((2, TP)),
        dma((2,)),
        dma((2,)),
        dma((ny, 2)),
        dma((ny, 2)),
        dma((nz, 2)),
        dma((nz, 2)),
        dma((2,)),
        dma((2,)),
        dma((2,)),
        dma((2,)),
        dma((TP,)),
        dma((TP,)),
        dma((TP,)),
        dma((TP,)),
    ]
    return pl.pallas_call(
        functools.partial(kernel, ny, nz),
        out_shape=jax.ShapeDtypeStruct((ch, model), BF16),
        in_specs=[
            hbm,
            vmem,
            hbm,
            hbm,
            hbm,
            hbm,
            hbm,
            vmem,
            vmem,
            smem,
            vmem,
            vmem,
            vmem,
            vmem,
            smem,
            vmem,
            vmem,
            vmem,
            hbm,
            hbm,
        ],
        out_specs=vmem,
        scratch_shapes=scratch,
        compiler_params=pltpu.CompilerParams(
            collective_id=0, has_side_effects=True, vmem_limit_bytes=60 * 2**20
        ),
    )(
        tokens,
        input_norm_gain.reshape(1, model),
        pooling_input_matrix,
        query_projection_matrix,
        key_projection_matrix,
        value_projection_matrix,
        output_gate_matrix,
        input_gate_matrix.transpose(1, 2, 0),
        forget_gate_matrix.transpose(1, 2, 0),
        forget_gate_bias,
        log_forget_scale,
        extra_log_forget,
        starting_memory,
        starting_normalizer,
        starting_log_scale,
        pooling_group_map,
        pooling_channel_scale.reshape(1, -1),
        memory_head_gain.reshape(1, -1),
        pooling_output_matrix,
        memory_output_matrix,
    )


def solution(mesh):
    chips = mesh.shape["sp"] // 2
    ny = math.isqrt(chips) if math.isqrt(chips) ** 2 == chips else chips
    nz = chips // ny
    placed = (
        P("sp", "tp"),
        P(),
        P(None, "tp"),
        P(None, "tp"),
        P(None, "tp"),
        P(None, "tp"),
        P(None, "tp"),
        P(),
        P(),
        P(),
        P(None, "sp"),
        P(None, "sp"),
        P(None, "tp", None, None),
        P(None, "tp", None),
        P(None, "tp"),
        P(),
        P(),
        P(),
        P(),
        P(),
    )
    return jax.shard_map(
        functools.partial(per_device, ny, nz),
        mesh=mesh,
        in_specs=placed,
        out_specs=P(("sp", "tp"), None),
        check_vma=False,
    )
```

time: 390 us -> 75.1 us (0.19); the launches traced: 384 us -> 74.9 us
  matrix products: 134 us -> 0 us
  blocking collectives: 86.9 us -> 0 us
  Pallas kernels: 0 us -> 72.6 us
  local copies, waits for them, and re-layouts: 71.2 us -> 2.3 us
  waiting for transfers between devices: 44.1 us -> 0 us
  other arithmetic: 26.8 us -> 0 us
  between operations: 14 us -> 0.01 us
  starting transfers between devices: 5.59 us -> 0 us
    dot_general x109 -> x0, matrix products: 134 us -> none  [the longest x16 21.4 us: block_step(): jnp.einsum('hts,hsv->htv', scores, v_blk)]
    pallas_call x0 -> x1, Pallas kernels: none -> 72.6 us  [per_device(): pl.pallas_call(functools.partial(kernel, ny, nz), out_shape=jax.ShapeDtyp...]
    all_gather x3 -> x0, blocking collectives: 71.4 us -> none  [per_device(): gathered = lax.all_gather(stacked, 'sp', axis=0, tiled=True)]
    all_gather x2 -> x0, waiting for transfers between devices: 43.3 us -> none  [the longest x1 43.3 us: per_device(): whole_rows = lax.all_gather(tokens, 'tp', axis=1, tiled=True)]
    rev x6 -> x0, local copies, waits for them, and re-layouts: 29.2 us -> none  [the longest x1 9.37 us: per_device(): hidden = forward + backward[:, ::-1]]
    all_to_all x1 -> x0, blocking collectives: 15.5 us -> none  [per_device(): owned = lax.all_to_all(mixed, 'tp', split_axis=0, concat_axis=1, tiled=True)]
    reshape x7 -> x0, local copies, waits for them, and re-layouts: 11.3 us -> none  [the longest x2 4.74 us: from_blocks(): jnp.moveaxis(source, 0, 1)]
    another operation x24 -> x0, other arithmetic: 7.26 us -> none  [the longest x16 4.95 us: block_step(): cumulative = jnp.cumsum(f_blk, axis=-1)]
  transfers between devices with their start and end apart: 4 -> 0, of which waited for: 1 -> 0; matrix products, arithmetic and copies ran while one was open for 8% -> 0% of each run, Pallas kernels for 0% -> 0%
where the time goes in v1:
time: 75.1 us; the launch traced here: 74.9 us
  Pallas kernels  72.6 us (97%)
  local copies, waits for them, and re-layouts  2.3 us (3%)
    pallas_call x1, Pallas kernels, per_device(): pl.pallas_call(functools.partial(kernel, ny, nz), out_shape=jax.ShapeDtyp...  72.6 us
    unnamed x1, local copies, waits for them, and re-layouts  2.3 us

profile of v1, /device:TPU:1, one launch (start us, length us, event | category | flops | bytes accessed | tf_op | source)
XLA Modules:
  0.0 74.9 jit_solution(5177928497128678456)
XLA Ops:
  0.0 72.6 %shard_map.190 = bf16[256,2048]{1,0:T(8,128)(2,1)} custom-call(bf16[1024,512]{1,0:T(8,128)(2,1)} %tok.1, f32[1,2048]{1,0:T(1,128)} %bitcast.7, bf16[2048,128]{1,0:T(8,128)(2,1)} %wp_hbm.1, bf16[2048,256]{1,0:T(8,128)(2,1)} %wq_hbm.1, bf16[2048,256]{1,0:T(8,128)(2,1)} %wk_hbm.1, bf16[2048,256]{1,0:T(8,128)(2,1)} %wv_hbm.1, bf16[2048,256]{1,0:T(8,128)(2,1)} %wo_hbm.1, ...), custom_call_target="tpu_custom_call" | custom-call | tf_op jit(solution)/shard_map/pallas_call | solution.py:812
  72.6 2.3 %copy.22 = bf16[256,2048]{1,0:T(8,128)(2,1)} copy(bf16[256,2048]{1,0:T(8,128)(2,1)} %shard_map.190) | data formatting | bytes 2097152

commit v2 on v1

--- a/solution.py
+++ b/solution.py
@@ -11,6 +11,7 @@
 DH = 128
 EXT = 144
 TP = 4
+NCH = 8
 MARGIN = 64
 RIM = 16
 NEG_BIG = -1e30
@@ -81,6 +82,7 @@
     pool,
     gt,
     gsc,
+    ac,
     tri,
     xl,
     ar,
@@ -131,7 +133,8 @@
     rows = tok.shape[0]
     width = tok.shape[1]
     ch = rows // TP
-    hf = ch // 2
+    cr = rows // NCH
+    hf = cr // 2
     t = lax.axis_index("tp")
     s = lax.axis_index("sp")
     ns = 2 * ny * nz
@@ -175,7 +178,7 @@
     pl.semaphore_wait(barrier, len(peers))
 
     def own_copy(c, way):
-        span = pl.ds(pl.multiple_of(c * ch, ch), ch)
+        span = pl.ds(pl.multiple_of(c * cr, cr), cr)
         return pltpu.make_async_remote_copy(
             src_ref=tok.at[span],
             dst_ref=xg.at[t, span],
@@ -186,7 +189,7 @@
         )
 
     def fwd_copy(c, way):
-        span = pl.ds(pl.multiple_of(c * ch + way * hf, hf), hf)
+        span = pl.ds(pl.multiple_of(c * cr + way * hf, hf), hf)
         slot = left if way == 0 else right
         return pltpu.make_async_remote_copy(
             src_ref=xg.at[slot, span],
@@ -223,21 +226,94 @@
     for one in loads[:5]:
         one.wait()
 
+    def project_state(c):
+        span = pl.ds(pl.multiple_of(c * cr, cr), cr)
+        normed = nb[...]
+        gsc[:, span] = dot_t(gt[...], normed)
+        ks[span] = dot(normed, wk[...]).astype(BF16)
+        v_all = dot(normed, wv[...]).astype(BF16).astype(F32).T.astype(BF16)
+        for h in range(2):
+            vt[h, 0:DH, span] = v_all[h * DH : (h + 1) * DH]
+
+    def project_rest(c):
+        base = pl.multiple_of(c * cr, cr)
+        span = pl.ds(base, cr)
+        normed = nb[...]
+        qs[span] = dot(normed, wq[...]).astype(BF16)
+        og[span] = dot(normed, wo[...]).astype(BF16)
+        pool[pl.ds(pl.multiple_of(base + MARGIN, MARGIN), cr)] = dot(normed, wp[...]).astype(BF16)
+
+    def state_part(b):
+        span = pl.ds(pl.multiple_of(b * ch, ch), ch)
+        ins = []
+        fgs = []
+        for r in range(2):
+            for h in range(2):
+                ins.append(gsc[pl.ds(8 * r + 2 * t + h, 1), span])
+                x = gsc[pl.ds(16 + 8 * r + 2 * t + h, 1), span] + bias[r, 2 * t + h]
+                fgs.append(
+                    (jnp.minimum(x, 0.0) - jnp.log1p(jnp.exp(-jnp.abs(x)))) * fscale[r : r + 1, span]
+                    + fextra[r : r + 1, span]
+                )
+        blank = jnp.zeros((4, ch), F32)
+        log_in = jnp.concatenate(ins + [blank], axis=0)
+        log_fg = jnp.concatenate(fgs + [blank], axis=0)
+        high = log_fg.astype(BF16).astype(F32)
+        rest = log_fg - high
+        mid = rest.astype(BF16).astype(F32)
+        low = rest - mid
+        parts = jnp.concatenate([high, mid, low, jnp.zeros((8, ch), F32)], axis=0).astype(BF16)
+        sums = dot(parts, tri[...])
+        sums = sums[0:8] + sums[8:16] + sums[16:24]
+        which = lax.broadcasted_iota(jnp.int32, (8, ch), 0)
+        falls = jnp.where(which < 2, sums[:, 0:ch], sums[:, ch : 2 * ch])
+        a_row = log_in - falls
+        ac[span] = jnp.concatenate([a_row, jnp.zeros((DH - 8, ch), F32)], axis=0).T
+        peak = jnp.max(a_row, axis=1, keepdims=True)
+        weight = jnp.exp(a_row - peak + half_log)
+        ends = jnp.where(which[:, 0:1] < 2, falls[:, ch - 1 : ch], falls[:, 0:1])
+        bs[b] = jnp.broadcast_to(ends, (8, DH))
+        ms[b] = jnp.broadcast_to(ends + peak, (8, DH))
+        for h in range(2):
+            k_h = ks[span, h * DH : (h + 1) * DH]
+            v_ext = vt[h, :, span].astype(F32)
+            for r in range(2):
+                ci = 2 * r + h
+                cst[b, ci] = dot((v_ext * weight[ci : ci + 1]).astype(BF16), k_h)
+
+    def output_part(b):
+        span = pl.ds(pl.multiple_of(b * ch, ch), ch)
+        rr = lax.broadcasted_iota(jnp.int32, (ch, ch), 0)
+        cc = lax.broadcasted_iota(jnp.int32, (ch, ch), 1)
+        for h in range(2):
+            k_h = ks[span, h * DH : (h + 1) * DH]
+            q_h = qs[span, h * DH : (h + 1) * DH]
+            scores = dot_t(k_h, q_h)
+            v_ext = vt[h, :, span]
+            for r in range(2):
+                ci = 2 * r + h
+                inside = (rr <= cc) if r == 0 else (rr >= cc)
+                expo = jnp.where(inside, ac[span, ci : ci + 1], NEG_BIG)
+                top = jnp.max(expo, axis=0, keepdims=True)
+                probs = (scores * jnp.exp(expo - top + half_log)).astype(BF16)
+                xl[ci, :, span] = dot(v_ext, probs)
+                ar[pl.ds(ci, 1), span] = top
+
     def chunk(c, carry):
-        @pl.when(c + 1 < TP)
+        @pl.when(c + 1 < NCH)
         def _():
             for way in (0, 1):
                 own_copy(c + 1, way).wait_recv()
                 fwd_copy(c + 1, way).start()
 
-        @pl.when(c + 3 < TP)
+        @pl.when(c + 3 < NCH)
         def _():
             for way in (0, 1):
                 own_copy(c + 3, way).start()
 
         for way in (0, 1):
             slot = left if way == 0 else right
-            span = pl.ds(pl.multiple_of(c * ch + way * hf, hf), hf)
+            span = pl.ds(pl.multiple_of(c * cr + way * hf, hf), hf)
             far = lax.rem(t + 2, TP)
             pltpu.make_async_remote_copy(
                 src_ref=xg.at[far, span],
@@ -248,8 +324,7 @@
                 device_id_type=MESH,
             ).wait_recv()
 
-        base = pl.multiple_of(c * ch, ch)
-        span = pl.ds(base, ch)
+        base = pl.multiple_of(c * cr, cr)
         sub = 64
 
         def norm(i, carry):
@@ -276,67 +351,24 @@
                     ).astype(BF16)
             return carry
 
-        lax.fori_loop(0, ch // sub, norm, 0)
-        normed = nb[...]
-        gsc[...] = dot_t(gt[...], normed)
-        k_all = dot(normed, wk[...]).astype(BF16)
-        q_all = dot(normed, wq[...]).astype(BF16)
-        v_all = dot(normed, wv[...]).astype(BF16).astype(F32).T.astype(BF16)
-        ks[span] = k_all
-        qs[span] = q_all
-        og[span] = dot(normed, wo[...]).astype(BF16)
-        pool[pl.ds(pl.multiple_of(base + MARGIN, MARGIN), ch)] = dot(normed, wp[...]).astype(BF16)
-        for h in range(2):
-            vt[h, 0:DH, span] = v_all[h * DH : (h + 1) * DH]
-
-        ins = []
-        fgs = []
-        for r in range(2):
-            for h in range(2):
-                ins.append(gsc[pl.ds(8 * r + 2 * t + h, 1), :])
-                x = gsc[pl.ds(16 + 8 * r + 2 * t + h, 1), :] + bias[r, 2 * t + h]
-                fgs.append(
-                    (jnp.minimum(x, 0.0) - jnp.log1p(jnp.exp(-jnp.abs(x)))) * fscale[r : r + 1, span]
-                    + fextra[r : r + 1, span]
-                )
-        blank = jnp.zeros((4, ch), F32)
-        log_in = jnp.concatenate(ins + [blank], axis=0)
-        log_fg = jnp.concatenate(fgs + [blank], axis=0)
-        high = log_fg.astype(BF16).astype(F32)
-        rest = log_fg - high
-        mid = rest.astype(BF16).astype(F32)
-        low = rest - mid
-        parts = jnp.concatenate([high, mid, low, jnp.zeros((8, ch), F32)], axis=0).astype(BF16)
-        sums = dot(parts, tri[...])
-        sums = sums[0:8] + sums[8:16] + sums[16:24]
-        which = lax.broadcasted_iota(jnp.int32, (8, ch), 0)
-        falls = jnp.where(which < 2, sums[:, 0:ch], sums[:, ch : 2 * ch])
-        a_row = log_in - falls
-        a_col = jnp.concatenate([a_row, jnp.zeros((DH - 8, ch), F32)], axis=0).T
-        peak = jnp.max(a_row, axis=1, keepdims=True)
-        weight = jnp.exp(a_row - peak + half_log)
-        ends = jnp.where(which[:, 0:1] < 2, falls[:, ch - 1 : ch], falls[:, 0:1])
-        bs[c] = jnp.broadcast_to(ends, (8, DH))
-        ms[c] = jnp.broadcast_to(ends + peak, (8, DH))
-        rr = lax.broadcasted_iota(jnp.int32, (ch, ch), 0)
-        cc = lax.broadcasted_iota(jnp.int32, (ch, ch), 1)
-        for h in range(2):
-            k_h = k_all[:, h * DH : (h + 1) * DH]
-            q_h = q_all[:, h * DH : (h + 1) * DH]
-            scores = dot_t(k_h, q_h)
-            v_ext = vt[h, :, span]
-            for r in range(2):
-                ci = 2 * r + h
-                inside = (rr <= cc) if r == 0 else (rr >= cc)
-                expo = jnp.where(inside, a_col[:, ci : ci + 1], NEG_BIG)
-                top = jnp.max(expo, axis=0, keepdims=True)
-                probs = (scores * jnp.exp(expo - top + half_log)).astype(BF16)
-                xl[ci, :, span] = dot(v_ext, probs)
-                ar[pl.ds(ci, 1), span] = top
-                cst[c, ci] = dot((v_ext.astype(F32) * weight[ci : ci + 1]).astype(BF16), k_h)
+        lax.fori_loop(0, cr // sub, norm, 0)
+        project_state(c)
+
+        @pl.when(c + 1 < NCH)
+        def _():
+            project_rest(c)
+
+        @pl.when(lax.rem(c, 2) == 1)
+        def _():
+            state_part(c // 2)
+
+        @pl.when((lax.rem(c, 2) == 0) & (c > 0))
+        def _():
+            output_part(c // 2 - 1)
+
         return carry
 
-    lax.fori_loop(0, TP, chunk, 0)
+    lax.fori_loop(0, NCH, chunk, 0)
 
     to_prev = pltpu.make_async_remote_copy(
         src_ref=pool.at[pl.ds(MARGIN, RIM)],
@@ -381,6 +413,7 @@
     swap = pair(sum_c.at[1 - core], sum_s.at[1 - core], r0_c, r0_s, r0_ss, r0_rs, (partner, t))
     for one in swap:
         one.start()
+    project_rest(NCH - 1)
 
     @pl.when(s > 0)
     def _():
@@ -414,6 +447,8 @@
     for j in range(1, ny):
         for one in y_pair(j, yi):
             one.start()
+
+    output_part(TP - 1)
 
     @pl.when(s < ns - 1)
     def _():
@@ -684,7 +719,7 @@
         ).wait_recv()
         mem_part(src, j == 2)
 
-    for c in range(TP):
+    for c in range(NCH):
         for way in (0, 1):
             own_copy(c, way).wait_send()
             fwd_copy(c, way).wait_send()
@@ -713,6 +748,10 @@
         blk = lax.rem(t + j, TP)
         pool_copy(blk, j).wait_send()
         mem_copy(blk, j).wait_send()
+
+
+def far(x):
+    return pltpu.with_memory_space_constraint(x, pltpu.HBM)
 
 
 def per_device(ny, nz, *args):
@@ -743,7 +782,7 @@
     ch = rows // TP
     vmem = pl.BlockSpec(memory_space=pltpu.VMEM)
     smem = pl.BlockSpec(memory_space=pltpu.SMEM)
-    hbm = pl.BlockSpec(memory_space=pl.ANY)
+    hbm = pl.BlockSpec(memory_space=pltpu.HBM)
     dma = pltpu.SemaphoreType.DMA
     scratch = [
         pltpu.VMEM((TP, rows, width), BF16),
@@ -754,14 +793,15 @@
         pltpu.VMEM((model, 2 * DH), BF16),
         pltpu.VMEM(pooling_output_matrix.shape, BF16),
         pltpu.VMEM(memory_output_matrix.shape, BF16),
-        pltpu.VMEM((ch, model), BF16),
+        pltpu.VMEM((rows // NCH, model), BF16),
         pltpu.VMEM((rows, 2 * DH), BF16),
         pltpu.VMEM((rows, 2 * DH), BF16),
         pltpu.VMEM((2, EXT, rows), BF16),
         pltpu.VMEM((rows, 2 * DH), BF16),
         pltpu.VMEM((rows + 2 * MARGIN, DH), BF16),
         pltpu.VMEM((32, model), BF16),
-        pltpu.VMEM((32, ch), F32),
+        pltpu.VMEM((32, rows), F32),
+        pltpu.VMEM((rows, DH), F32),
         pltpu.VMEM((ch, 2 * ch), BF16),
         pltpu.VMEM((4, EXT, rows), F32),
         pltpu.VMEM((8, rows), F32),
@@ -790,10 +830,10 @@
         pltpu.VMEM((TP, ch, 2 * DH), BF16),
         pltpu.VMEM((ch, model), F32),
         dma((8,)),
-        dma((2, TP)),
-        dma((2, TP)),
-        dma((2, TP)),
-        dma((2, TP)),
+        dma((2, NCH)),
+        dma((2, NCH)),
+        dma((2, NCH)),
+        dma((2, NCH)),
         dma((2,)),
         dma((2,)),
         dma((ny, 2)),
@@ -837,29 +877,29 @@
         out_specs=vmem,
         scratch_shapes=scratch,
         compiler_params=pltpu.CompilerParams(
-            collective_id=0, has_side_effects=True, vmem_limit_bytes=60 * 2**20
+            collective_id=0, has_side_effects=True, vmem_limit_bytes=44 * 2**20
         ),
     )(
-        tokens,
-        input_norm_gain.reshape(1, model),
-        pooling_input_matrix,
-        query_projection_matrix,
-        key_projection_matrix,
-        value_projection_matrix,
-        output_gate_matrix,
-        input_gate_matrix.transpose(1, 2, 0),
-        forget_gate_matrix.transpose(1, 2, 0),
-        forget_gate_bias,
-        log_forget_scale,
-        extra_log_forget,
-        starting_memory,
-        starting_normalizer,
-        starting_log_scale,
-        pooling_group_map,
-        pooling_channel_scale.reshape(1, -1),
-        memory_head_gain.reshape(1, -1),
-        pooling_output_matrix,
-        memory_output_matrix,
+        far(tokens),
+        far(input_norm_gain.reshape(1, model)),
+        far(pooling_input_matrix),
+        far(query_projection_matrix),
+        far(key_projection_matrix),
+        far(value_projection_matrix),
+        far(output_gate_matrix),
+        far(input_gate_matrix.transpose(1, 2, 0)),
+        far(forget_gate_matrix.transpose(1, 2, 0)),
+        far(forget_gate_bias),
+        far(log_forget_scale),
+        far(extra_log_forget),
+        far(starting_memory),
+        far(starting_normalizer),
+        far(starting_log_scale),
+        far(pooling_group_map),
+        far(pooling_channel_scale.reshape(1, -1)),
+        far(memory_head_gain.reshape(1, -1)),
+        far(pooling_output_matrix),
+        far(memory_output_matrix),
     )
 
 

time: 75.1 us -> 72.3 us (0.963)
  Pallas kernels: 72.6 us -> 71.2 us
  local copies, waits for them, and re-layouts: 2.3 us -> 0.97 us
    pallas_call x1, Pallas kernels: 72.6 us -> 71.2 us  [per_device(): pl.pallas_call(functools.partial(kernel, ny, nz), out_shape=jax.ShapeDtyp...]
    unnamed x1, local copies, waits for them, and re-layouts: 2.3 us -> 0.97 us
where the time goes in v2:
time: 72.3 us; the launch traced here: 72.2 us
  Pallas kernels  71.2 us (98%)
  local copies, waits for them, and re-layouts  0.97 us (1%)
    pallas_call x1, Pallas kernels, per_device(): pl.pallas_call(functools.partial(kernel, ny, nz), out_shape=jax.ShapeDtyp...  71.2 us

profile of v2, /device:TPU:1, one launch (start us, length us, event | category | flops | bytes accessed | tf_op | source)
XLA Modules:
  0.0 72.2 jit_solution(9951144262322530820)
XLA Ops:
  0.0 71.2 %shard_map.190 = bf16[256,2048]{1,0:T(8,128)(2,1)S(1)} custom-call(bf16[1024,512]{1,0:T(8,128)(2,1)} %tok.1, f32[1,2048]{1,0:T(1,128)} %bitcast.7, bf16[2048,128]{1,0:T(8,128)(2,1)} %wp_hbm.1, bf16[2048,256]{1,0:T(8,128)(2,1)} %wq_hbm.1, bf16[2048,256]{1,0:T(8,128)(2,1)} %wk_hbm.1, bf16[2048,256]{1,0:T(8,128)(2,1)} %wv_hbm.1, bf16[2048,256]{1,0:T(8,128)(2,1)} %wo_hbm.1, ...), custom_call_target="tpu_custom_call" | custom-call | tf_op jit(solution)/shard_map/pallas_call | solution.py:852
  71.3 1.0 %copy.22 = bf16[256,2048]{1,0:T(8,128)(2,1)} copy(bf16[256,2048]{1,0:T(8,128)(2,1)S(1)} %shard_map.190) | data formatting | bytes 2097152
